TPU v7x, 32 devices: a whole 2x2x4 slice. The times are simulated.
32 devices in a mesh: ra: 8 (over z, y), cb: 4 (over x, core).
Axes of the slice: x: 2, y: 2, z: 4, core: 2. Of those that a mesh axis runs over, the one named last changes fastest.
Arguments:
- tokens: bfloat16 [1024, 4096], P(None, 'ra'), may hold values from -40 to 40
- norm_gain: float32 [4096], P('ra'), may hold values from 0.1 to 1.9
- gate_weight: bfloat16 [4096, 11264], P('ra', 'cb'), may hold values from -0.09375 to 0.09375
- up_weight: bfloat16 [4096, 11264], P('ra', 'cb'), may hold values from -0.09375 to 0.09375
- down_weight: bfloat16 [11264, 4096], P('cb', 'ra'), may hold values from -0.0546875 to 0.0546875
- out_gain: float32 [4096], P('ra'), may hold values from 0.1 to 1.9
Outputs:
- normed: bfloat16 [1024, 4096], P(None, 'ra')
All inputs are finite; a program needn't handle non-finite values.
Results may differ from a plain program's by a relative error of at most 0.0076.
Values may be sent and summed in bfloat16 or wider, within the bound.
No kernel may reach another device: no remote copies, remote signals or barrier semaphores. Data moves between devices by JAX's collectives and lax.ppermute only.
A program may use at most 128 MiB of HBM per device.

v0:
```python
import jax
import jax.numpy as jnp
from jax import lax
from jax.sharding import PartitionSpec as P

D = 4096


def body(tokens, norm_gain, gate_weight, up_weight, down_weight, out_gain):
    stream_in = tokens.astype(jnp.float32)
    local_sq = jnp.sum(stream_in * stream_in, axis=1)
    scaled = (stream_in * norm_gain[None, :]).astype(jnp.bfloat16)
    gate_part = jnp.dot(scaled, gate_weight, preferred_element_type=jnp.float32)
    up_part = jnp.dot(scaled, up_weight, preferred_element_type=jnp.float32)
    gate_sum, up_sum, sq_sum = (
        lax.psum_scatter(gate_part, "ra", scatter_dimension=0, tiled=True),
        lax.psum_scatter(up_part, "ra", scatter_dimension=0, tiled=True),
        lax.psum_scatter(local_sq, "ra", scatter_dimension=0, tiled=True),
    )
    inv_rms = jax.lax.rsqrt(sq_sum / D + 1e-06)[:, None]
    hidden = (jax.nn.silu(gate_sum * inv_rms) * (up_sum * inv_rms)).astype(jnp.bfloat16)
    down_part = jnp.dot(
        lax.all_gather(hidden, "ra", axis=0, tiled=True),
        down_weight,
        preferred_element_type=jnp.float32,
    )
    branch = lax.psum(down_part, "cb")
    stream = 0.5 * stream_in + branch
    total_sq = lax.psum(jnp.sum(stream * stream, axis=1), "ra")
    factor = jax.lax.rsqrt(total_sq / D + 1e-06)[:, None]
    return (stream * factor * out_gain[None, :]).astype(jnp.bfloat16)


def solution(mesh):
    placed = (P(None, "ra"), P("ra"), P("ra", "cb"), P("ra", "cb"), P("cb", "ra"), P("ra"))
    return jax.shard_map(body, mesh=mesh, in_specs=placed, out_specs=P(None, "ra"), check_vma=False)
```

profile of v0, /device:TPU:0, one launch (start us, length us, event | category | flops | bytes accessed | tf_op | source)
XLA Modules:
  0.0 593.5 jit_solution(14529803967618089035)
XLA Ops:
  6.5 0.0 copy-start
  6.5 0.0 reduce-scatter.3.cloned.1.call-start
  6.5 1.8 copy-done
  8.4 7.5 %fusion.5 = f32[1024,2816]{1,0:T(8,128)} fusion(bf16[512,2816]{1,0:T(8,128)(2,1)S(1)} %copy-done, bf16[1024,512]{1,0:T(8,128)(2,1)} %param.6, f32[512]{0:T(512)} %param.7), kind=kOutput, calls=%fused_computation.10 | convolution fusion | flops 2954362880 | bytes 15468544 | tf_op jit(solution)/shard_map/dot_general | solution.py:13
  15.8 0.0 copy-start.2
  15.8 0.0 reduce-scatter.3.cloned.1.call-update
  15.9 0.0 reduce-scatter.5.cloned.1.call-start
  15.9 0.6 copy-done.2
  16.5 9.9 %fusion.3 = f32[1024,2816]{1,0:T(8,128)} fusion(bf16[512,2816]{1,0:T(8,128)(2,1)} %param.9, bf16[1024,512]{1,0:T(8,128)(2,1)} %param.6, f32[512]{0:T(512)S(1)} %copy-done.2), kind=kOutput, calls=%fused_computation.9 | convolution fusion | flops 2954362880 | bytes 15468544 | tf_op jit(solution)/shard_map/dot_general | solution.py:14
  26.4 0.0 copy-start.3
  26.4 0.0 reduce-scatter.5.cloned.1.call-update
  26.4 0.0 all-gather.2.cloned.1.call-start
  26.5 0.6 copy-done.3
  27.0 0.6 dynamic-slice
  28.3 1.5 fusion.2
  29.8 24.5 %all-reduce = f32[1024]{0:T(1024)S(1)} all-reduce(f32[1024]{0:T(1024)S(1)} %fusion.2), channel_id=3, replica_groups=mesh['ra'=8,'cb'=4] {'ra'}, use_global_device_ids=true, to_apply=%region_2.0.clone | all-reduce | flops 1024 | bytes 8192
  54.3 0.1 fusion.8
  54.4 157.7 %reduce-scatter.3.cloned.1.call-done = f32[128,2816]{1,0:T(8,128)} async-done(((f32[1024,2816]{1,0:T(8,128)}), f32[128,2816]{1,0:T(8,128)}) %reduce-scatter.3.cloned.1.call-update) | async-done | bytes 1441808 | tf_op jit(solution)/shard_map/reduce_scatter | solution.py:16
  212.1 195.6 %reduce-scatter.5.cloned.1.call-done = f32[128,2816]{1,0:T(8,128)} async-done(((f32[1024,2816]{1,0:T(8,128)}), f32[128,2816]{1,0:T(8,128)}) %reduce-scatter.5.cloned.1.call-update) | async-done | bytes 1441808 | tf_op jit(solution)/shard_map/reduce_scatter | solution.py:17
  407.7 3.1 multiply_convert_fusion.1
  410.8 0.0 all-gather.2.cloned.1.call-update
  410.8 0.0 all-reduce.3.cloned.1.call-start
  410.9 91.5 %all-gather.2.cloned.1.call-done = bf16[1024,2816]{1,0:T(8,128)(2,1)} async-done(((bf16[128,2816]{1,0:T(8,128)(2,1)}), bf16[1024,2816]{1,0:T(8,128)(2,1)}) %all-gather.2.cloned.1.call-update) | async-done | bytes 5767184 | tf_op jit(solution)/shard_map/all_gather | solution.py:23
  502.4 8.0 %fusion.9 = f32[1024,512]{1,0:T(8,128)} fusion(bf16[1024,2816]{1,0:T(8,128)(2,1)} %all-gather.2.cloned.1.call-done, bf16[2816,512]{1,0:T(8,128)(2,1)} %param.10), kind=kOutput, calls=%fused_computation.15 | convolution fusion | flops 2952790016 | bytes 10747904 | tf_op jit(solution)/shard_map/dot_general | solution.py:22
  510.4 0.0 all-reduce.3.cloned.1.call-update
  510.4 0.0 copy-start.1
  510.4 49.7 %all-reduce.3.cloned.1.call-done = f32[1024,512]{1,0:T(8,128)} async-done(((f32[1024,512]{1,0:T(8,128)}), f32[1024,512]{1,0:T(8,128)}) %all-reduce.3.cloned.1.call-update) | async-done | bytes 2097168 | tf_op jit(solution)/shard_map/psum | solution.py:27
  560.1 2.3 multiply_reduce_fusion
  562.4 21.4 %psum.15 = f32[1024]{0:T(1024)S(1)} all-reduce(f32[1024]{0:T(1024)S(1)} %multiply_reduce_fusion), channel_id=1, replica_groups=mesh['ra'=8,'cb'=4] {'ra'}, use_global_device_ids=true, to_apply=%region_6.7 | all-reduce | flops 1024 | bytes 8192 | tf_op jit(solution)/shard_map/psum | solution.py:29
  583.7 0.0 copy-done.1
  583.7 3.2 multiply_convert_fusion
  (1 shorter events, 0.0 us)
Async XLA Ops:
  6.5 1.8 copy-start
  6.5 205.6 %reduce-scatter.3.cloned.1.call-start = ((), (), s32[]{:S(2)}) async-start(), calls=%async_computation.2 | async-start | bytes 12976128 | tf_op jit(solution)/shard_map/reduce_scatter | solution.py:16
  15.8 0.7 copy-start.2
  15.9 391.8 %reduce-scatter.5.cloned.1.call-start = ((), (), s32[]{:S(2)}) async-start(), calls=%async_computation.3 | async-start | bytes 12976128 | tf_op jit(solution)/shard_map/reduce_scatter | solution.py:17
  26.4 0.7 copy-start.3
  26.4 476.0 %all-gather.2.cloned.1.call-start = ((), (), s32[]{:S(2)}) async-start(), calls=%async_computation.4 | async-start | bytes 6488064 | tf_op jit(solution)/shard_map/all_gather | solution.py:23
  410.8 149.3 %all-reduce.3.cloned.1.call-start = ((), (), s32[]{:S(2)}) async-start(), calls=%async_computation.5 | async-start | bytes 4194304 | tf_op jit(solution)/shard_map/psum | solution.py:27
  510.4 73.4 %copy-start.1 = (f32[512]{0:T(512)S(1)}, f32[512]{0:T(512)}, u32[]{:S(2)}) copy-start(f32[512]{0:T(512)} %param.11) | copy-start | bytes 6148
Sparse Core Ops, SparseCore 0:
  16.0 196.0 reduce-scatter.2
  215.7 191.9 reduce-scatter.4
  410.9 91.4 all-gather.1
  510.5 49.5 all-reduce.2
where the time goes:
time: 594 us; the launch traced here: 593 us
  waiting for transfers between devices  495 us (83%)
  blocking collectives  45.9 us (8%)
  matrix products  25.3 us (4%)
  between operations  13.8 us (2%)
  other arithmetic  10.2 us (2%)
    reduce_scatter x1, waiting for transfers between devices, body(): lax.psum_scatter(up_part, 'ra', scatter_dimension=0, tiled=True)  196 us
    reduce_scatter x1, waiting for transfers between devices, body(): lax.psum_scatter(gate_part, 'ra', scatter_dimension=0, tiled=True)  158 us
    all_gather x1, waiting for transfers between devices, body(): lax.all_gather(hidden, 'ra', axis=0, tiled=True)  91.5 us
    psum x1, waiting for transfers between devices, body(): branch = lax.psum(down_part, 'cb')  49.7 us
    unnamed x1, blocking collectives  24.5 us
    psum x1, blocking collectives, body(): total_sq = lax.psum(jnp.sum(stream * stream, axis=1), 'ra')  21.4 us
  transfers between devices with their start and end apart: 4, of which 4 were waited for; matrix products, arithmetic and copies ran while one was open for 2% of the time, Pallas kernels for 0%

commit v1 on v0

--- a/solution.py
+++ b/solution.py
@@ -24,7 +24,26 @@
         down_weight,
         preferred_element_type=jnp.float32,
     )
-    branch = lax.psum(down_part, "cb")
+
+    def name_sites(own_rows):
+        how_many = lax.psum(1, axis_name="cb")
+
+        def convert_columns_on_mesh(local_next, val):
+            if val >= how_many:
+                return local_next
+            block_now = convert_columns_on_mesh(
+                local_next
+                + lax.ppermute(
+                    local_next, "cb", tuple(((num, num ^ val) for num in range(how_many)))
+                ),
+                2 * val,
+            )
+            return block_now
+
+        parts_out = convert_columns_on_mesh(own_rows, 1)
+        return parts_out
+
+    branch = name_sites(down_part)
     stream = 0.5 * stream_in + branch
     total_sq = lax.psum(jnp.sum(stream * stream, axis=1), "ra")
     factor = jax.lax.rsqrt(total_sq / D + 1e-06)[:, None]

time: 594 us -> 595 us (level)
    ppermute x0 -> x2, waiting for transfers between devices: none -> 50.3 us  [convert_columns_on_mesh(): lax.ppermute(local_next, 'cb', tuple(((num, num ^ val) for num in range(h...]
    psum x1 -> x0, waiting for transfers between devices: 49.7 us -> none  [body(): branch = lax.psum(down_part, 'cb')]
  transfers between devices with their start and end apart: 4 -> 5, of which waited for: 4 -> 5; matrix products, arithmetic and copies ran while one was open for 2% -> 2% of each run, Pallas kernels for 0% -> 0%
where the time goes in v1:
time: 595 us
  waiting for transfers between devices  495 us (83%)
  blocking collectives  43.5 us (7%)
  matrix products  23.5 us (4%)
  between operations  13.7 us (2%)
  other arithmetic  9.61 us (2%)
  local copies, waits for them, and re-layouts  7.19 us (1%)
    reduce_scatter x1, waiting for transfers between devices, body(): lax.psum_scatter(up_part, 'ra', scatter_dimension=0, tiled=True)  196 us
    reduce_scatter x1, waiting for transfers between devices, body(): lax.psum_scatter(gate_part, 'ra', scatter_dimension=0, tiled=True)  158 us
    all_gather x1, waiting for transfers between devices, body(): lax.all_gather(hidden, 'ra', axis=0, tiled=True)  91.6 us
    ppermute x2, waiting for transfers between devices, convert_columns_on_mesh(): lax.ppermute(local_next, 'cb', tuple(((num, num ^ val) for num in range(h...  50.3 us
    unnamed x1, blocking collectives  25 us
    psum x1, blocking collectives, body(): total_sq = lax.psum(jnp.sum(stream * stream, axis=1), 'ra')  18.6 us
  transfers between devices with their start and end apart: 5, of which 5 were waited for; matrix products, arithmetic and copies ran while one was open for 2% of the time, Pallas kernels for 0%

profile of v1, /device:TPU:0, one launch (start us, length us, event | category | flops | bytes accessed | tf_op | source)
XLA Modules:
  0.0 594.7 jit_solution(4166607993195009259)
XLA Ops:
  6.5 0.0 copy-start
  6.5 0.0 copy-start.5
  6.5 0.0 reduce-scatter.3.cloned.1.call-start
  6.5 2.4 copy.9
  9.0 0.0 copy-done
  9.0 0.0 copy-done.5
  9.0 7.7 %fusion.5 = f32[1024,2816]{1,0:T(8,128)} fusion(bf16[512,2816]{1,0:T(8,128)(2,1)S(1)} %copy-done, bf16[1024,512]{0,1:T(8,128)(2,1)} %copy.9, f32[512]{0:T(512)S(1)} %copy-done.5), kind=kOutput, calls=%fused_computation.10 | convolution fusion | flops 2954362880 | bytes 15468544 | tf_op jit(solution)/shard_map/dot_general | solution.py:13
  16.7 0.0 reduce-scatter.3.cloned.1.call-update
  16.7 0.0 reduce-scatter.5.cloned.1.call-start
  16.8 9.7 %fusion.3 = f32[1024,2816]{1,0:T(8,128)} fusion(bf16[512,2816]{1,0:T(8,128)(2,1)} %param.9, bf16[1024,512]{0,1:T(8,128)(2,1)} %copy.9, f32[512]{0:T(512)S(1)} %copy-done.5), kind=kOutput, calls=%fused_computation.9 | convolution fusion | flops 2954362880 | bytes 15468544 | tf_op jit(solution)/shard_map/dot_general | solution.py:14
  26.4 0.0 copy-start.6
  26.4 0.0 reduce-scatter.5.cloned.1.call-update
  26.5 0.0 all-gather.2.cloned.1.call-start
  26.5 0.6 copy-done.6
  27.1 0.6 dynamic-slice
  28.3 1.5 fusion.2
  29.7 25.0 %all-reduce = f32[1024]{0:T(1024)S(1)} all-reduce(f32[1024]{0:T(1024)S(1)} %fusion.2), channel_id=3, replica_groups=mesh['ra'=8,'cb'=4] {'ra'}, use_global_device_ids=true, to_apply=%region_2.0.clone | all-reduce | flops 1024 | bytes 8192
  54.7 0.1 fusion.8
  54.8 157.9 %reduce-scatter.3.cloned.1.call-done = f32[128,2816]{1,0:T(8,128)} async-done(((f32[1024,2816]{1,0:T(8,128)}), f32[128,2816]{1,0:T(8,128)}) %reduce-scatter.3.cloned.1.call-update) | async-done | bytes 1441808 | tf_op jit(solution)/shard_map/reduce_scatter | solution.py:16
  212.7 195.6 %reduce-scatter.5.cloned.1.call-done = f32[128,2816]{1,0:T(8,128)} async-done(((f32[1024,2816]{1,0:T(8,128)}), f32[128,2816]{1,0:T(8,128)}) %reduce-scatter.5.cloned.1.call-update) | async-done | bytes 1441808 | tf_op jit(solution)/shard_map/reduce_scatter | solution.py:17
  408.3 3.1 multiply_convert_fusion.1
  411.4 0.0 all-gather.2.cloned.1.call-update
  411.4 91.6 %all-gather.2.cloned.1.call-done = bf16[1024,2816]{1,0:T(8,128)(2,1)} async-done(((bf16[128,2816]{1,0:T(8,128)(2,1)}), bf16[1024,2816]{1,0:T(8,128)(2,1)}) %all-gather.2.cloned.1.call-update) | async-done | bytes 5767184 | tf_op jit(solution)/shard_map/all_gather | solution.py:23
  503.0 6.1 %fusion.9 = f32[1024,512]{0,1:T(8,128)S(1)} fusion(bf16[1024,2816]{1,0:T(8,128)(2,1)} %all-gather.2.cloned.1.call-done, bf16[2816,512]{1,0:T(8,128)(2,1)} %param.10), kind=kOutput, calls=%fused_computation.15 | convolution fusion | flops 2952790016 | bytes 10747904 | tf_op jit(solution)/shard_map/dot_general | solution.py:22
  509.1 0.0 copy-start.2
  509.1 0.1 collective-permute-start
  509.2 4.1 collective-permute-done
  513.4 0.4 add.36
  513.8 0.0 copy-start.1
  513.8 0.0 copy-start.4
  513.8 1.5 collective-permute-start.1
  515.3 46.2 %collective-permute-done.1 = f32[1024,512]{0,1:T(8,128)S(1)} collective-permute-done((f32[1024,512]{0,1:T(8,128)S(1)}, f32[1024,512]{0,1:T(8,128)S(1)}, u32[]{:S(2)}, u32[]{:S(2)}) %collective-permute-start.1) | collective-permute-done | bytes 2097184 | tf_op jit(solution)/shard_map/ppermute | solution.py:36
  561.5 0.0 copy-done.1
  561.5 0.0 copy-start.3
  561.5 1.3 copy-done.3
  562.8 0.0 copy-done.2
  562.8 0.6 multiply_reduce_fusion
  563.4 18.6 %psum.7 = f32[1024]{0:T(1024)S(1)} all-reduce(f32[1024]{0:T(1024)S(1)} %multiply_reduce_fusion), channel_id=1, replica_groups=mesh['ra'=8,'cb'=4] {'ra'}, use_global_device_ids=true, to_apply=%region_5.6 | all-reduce | flops 1024 | bytes 8192 | tf_op jit(solution)/shard_map/psum | solution.py:48
  582.0 0.0 copy-done.4
  582.0 3.9 multiply_convert_fusion
  585.9 2.3 copy.10
  (1 shorter events, 0.0 us)
Async XLA Ops:
  6.5 2.4 copy-start
  6.5 2.4 copy-start.5
  6.5 206.1 %reduce-scatter.3.cloned.1.call-start = ((), (), s32[]{:S(2)}) async-start(), calls=%async_computation.2 | async-start | bytes 12976128 | tf_op jit(solution)/shard_map/reduce_scatter | solution.py:16
  16.7 391.5 %reduce-scatter.5.cloned.1.call-start = ((), (), s32[]{:S(2)}) async-start(), calls=%async_computation.3 | async-start | bytes 12976128 | tf_op jit(solution)/shard_map/reduce_scatter | solution.py:17
  26.4 0.7 copy-start.6
  26.5 476.5 %all-gather.2.cloned.1.call-start = ((), (), s32[]{:S(2)}) async-start(), calls=%async_computation.4 | async-start | bytes 6488064 | tf_op jit(solution)/shard_map/all_gather | solution.py:23
  509.1 53.7 %copy-start.2 = (bf16[1024,512]{0,1:T(8,128)(2,1)S(1)}, bf16[1024,512]{0,1:T(8,128)(2,1)}, u32[]{:S(2)}) copy-start(bf16[1024,512]{0,1:T(8,128)(2,1)} %copy.9) | copy-start | bytes 3145732
  509.1 4.2 collective-permute-start
  513.8 47.8 %copy-start.1 = (f32[1024,512]{0,1:T(8,128)}, f32[1024,512]{0,1:T(8,128)S(1)}, u32[]{:S(2)}) copy-start(f32[1024,512]{0,1:T(8,128)S(1)} %add.36) | copy-start | bytes 6291460
  513.8 68.2 %copy-start.4 = (f32[512]{0:T(512)S(1)}, f32[512]{0:T(512)}, u32[]{:S(2)}) copy-start(f32[512]{0:T(512)} %param.11) | copy-start | bytes 6148
  513.8 47.7 %collective-permute-start.1 = (f32[1024,512]{0,1:T(8,128)S(1)}, f32[1024,512]{0,1:T(8,128)S(1)}, u32[]{:S(2)}, u32[]{:S(2)}) collective-permute-start(f32[1024,512]{0,1:T(8,128)S(1)} %add.36), channel_id=1, source_target_pairs={{0,2},{1,3},{2,0},{3,1},{4,6},{5,7},{6,4},{7,5},{8,10},{9,11},{10,... | collective-permute-start | bytes 6291464 | tf_op jit(solution)/shard_map/ppermute | solution.py:36
  561.5 1.3 copy-start.3
Sparse Core Ops, SparseCore 0:
  16.9 195.7 reduce-scatter.2
  216.3 191.9 reduce-scatter.4
  411.5 91.4 all-gather.1
